TPU v7x, 128 devices: a whole 4x4x4 slice. The times are simulated.
128 devices in a mesh: sp: 16 (over z, y), dp: 8 (over x, core).
Axes of the slice: x: 4, y: 4, z: 4, core: 2. Of those that a mesh axis runs over, the one named last changes fastest.
Arguments:
- tokens: bfloat16 [8, 4096, 2048], P('dp', 'sp'), may hold values from -6 to 6
- w_query: bfloat16 [2048, 2048], P('dp', 'sp'), may hold values from -0.125 to 0.125
- w_key: bfloat16 [2048, 1024], P('dp', 'sp'), may hold values from -0.125 to 0.125
- w_value: bfloat16 [2048, 1024], P('dp', 'sp'), may hold values from -0.125 to 0.125
- w_out: bfloat16 [2048, 2048], P('dp', 'sp'), may hold values from -0.25 to 0.25
- qk_gain: float32 [2, 128], replicated, may hold values from 0.9 to 24
Outputs:
- mixed_out: bfloat16 [8, 4096, 2048], P('dp', 'sp')
All inputs are finite; a program needn't handle non-finite values.
Results may differ from a plain program's by a relative error of at most 0.006.
The roundings to bfloat16 on the way count: a program that leaves them out, or rounds other values in their place, can miss the bound.
Values may be sent and summed in bfloat16 or wider, within the bound.
A program may use at most 64 MiB of HBM per device.

v0:
```python
import math
import jax
import jax.numpy as jnp
import numpy as np
from jax import lax
from jax.sharding import PartitionSpec as P

HQ = 16
KV = 8
HD = 128
GRID_W = 64
ROPE_BASE = 10000.0
EPS = 1e-06


def in_order(blocks, dim):
    blocks = jnp.moveaxis(blocks, 0, dim)
    shape = blocks.shape
    return blocks.reshape(*shape[:dim], shape[dim] * shape[dim + 1], *shape[dim + 2 :])


def sent_to_all(x, axis):
    copies = jnp.broadcast_to(x, (lax.axis_size(axis), *x.shape))
    return lax.all_to_all(copies, axis, split_axis=0, concat_axis=0, tiled=True)


def collect(x, axis, dim):
    return in_order(sent_to_all(x, axis), dim)


def angles(positions):
    quarter = jnp.arange(0, HD // 2, 2, dtype=jnp.float32)
    inv_freq = ROPE_BASE ** (-quarter / (HD // 2))
    row_pos = (positions // GRID_W).astype(jnp.float32)
    col_pos = (positions % GRID_W).astype(jnp.float32)
    angle_table = jnp.concatenate(
        [row_pos[:, None] * inv_freq, col_pos[:, None] * inv_freq], axis=1
    )
    return (jnp.cos(angle_table), jnp.sin(angle_table))


def prepare(raw_proj, gain_row, cosine, sine_table):
    normed = (
        raw_proj * lax.rsqrt(jnp.mean(raw_proj * raw_proj, axis=-1, keepdims=True) + EPS) * gain_row
    )
    pair_view = normed.reshape(raw_proj.shape[:-1] + (HD // 2, 2))
    first_half = pair_view[..., 0]
    second = pair_view[..., 1]
    cos_b = cosine[:, None, :]
    sin_b = sine_table[:, None, :]
    turned = jnp.stack(
        [first_half * cos_b - second * sin_b, first_half * sin_b + second * cos_b], axis=-1
    )
    return turned.reshape(raw_proj.shape).astype(jnp.bfloat16)


def attend_head(query_rows, key_rows, value_rows):
    seq_len = query_rows.shape[0]
    block_len = math.gcd(seq_len, 512)
    blocks = query_rows.reshape(seq_len // block_len, block_len, HD)

    def one_block(row_block):
        scores = jnp.dot(row_block, key_rows.T, preferred_element_type=jnp.float32) * HD ** (-0.5)
        top_score = jnp.max(scores, axis=1, keepdims=True)
        weights = jnp.exp(scores - top_score)
        row_total = jnp.sum(weights, axis=1, keepdims=True)
        probs_bf = (weights / row_total).astype(jnp.bfloat16)
        return jnp.dot(probs_bf, value_rows, preferred_element_type=jnp.float32).astype(
            jnp.bfloat16
        )

    return lax.map(one_block, blocks).reshape(seq_len, HD)


def project(own_rows, weight):
    col_full = collect(weight, "sp", 1)
    return jnp.dot(
        own_rows,
        lax.all_gather(col_full, "dp", axis=0, tiled=True),
        preferred_element_type=jnp.float32,
    )


def on_device(tokens, w_query, w_key, w_value, w_out, qk_gain):
    own_rows = tokens[0]
    n_seqdev = lax.axis_size("sp")
    tok_local = own_rows.shape[0]
    positions = lax.axis_index("sp") * tok_local + jnp.arange(tok_local, dtype=jnp.int32)
    cosine, sine_table = angles(positions)
    heads_dev = HQ // n_seqdev
    group_size = HQ // KV
    kv_dev = max(1, heads_dev // group_size)
    chosen = (np.arange(n_seqdev) * heads_dev // group_size)[:, None] + np.arange(kv_dev)[None, :]
    chosen = chosen.reshape(-1)
    key_all = prepare(
        project(own_rows, w_key).reshape(tok_local, KV, HD), qk_gain[1], cosine, sine_table
    )
    values = project(own_rows, w_value).astype(jnp.bfloat16).reshape(tok_local, KV, HD)
    key_send = key_all[:, chosen, :].reshape(tok_local, -1)
    value_send = values[:, chosen, :].reshape(tok_local, -1)
    raw_proj = project(own_rows, w_query).reshape(tok_local, HQ, HD)
    query_heads = lax.all_to_all(
        prepare(raw_proj, qk_gain[0], cosine, sine_table).reshape(tok_local, HQ * HD),
        "sp",
        split_axis=1,
        concat_axis=0,
        tiled=True,
    )
    key_heads = lax.all_to_all(key_send, "sp", split_axis=1, concat_axis=0, tiled=True)
    value_heads = lax.all_to_all(value_send, "sp", split_axis=1, concat_axis=0, tiled=True)
    outputs = attend_head(query_heads, key_heads[:, 0:HD], value_heads[:, 0:HD])
    token_rows = lax.all_to_all(outputs, "sp", split_axis=0, concat_axis=1, tiled=True)
    return project(token_rows, w_out).astype(jnp.bfloat16)[None]


def solution(mesh):
    in_specs = (
        P("dp", "sp", None),
        P("dp", "sp"),
        P("dp", "sp"),
        P("dp", "sp"),
        P("dp", "sp"),
        P(),
    )
    out_specs = P("dp", "sp", None)
    return jax.shard_map(
        on_device, mesh=mesh, in_specs=in_specs, out_specs=out_specs, check_vma=False
    )
```

profile of v0, /device:TPU:0, one launch (start us, length us, event | category | flops | bytes accessed | tf_op | source)
XLA Modules:
  0.0 289.2 jit_solution(16202396729736009710)
XLA Ops:
  7.5 19.6 %all_to_all.84 = bf16[16,256,64]{1,2,0:T(8,128)(2,1)} all-to-all(bf16[16,256,64]{1,2,0:T(8,128)(2,1)S(1)} %broadcast_in_dim.42), channel_id=1, replica_groups=mesh['sp'=16,'dp'=8] {'sp'}, dimensions={0} | all-to-all | bytes 1048576 | tf_op jit(solution)/shard_map/all_to_all | solution.py:24
  28.0 13.8 %all_to_all.85 = bf16[16,256,64]{1,2,0:T(8,128)(2,1)} all-to-all(bf16[16,256,64]{1,2,0:T(8,128)(2,1)S(1)} %broadcast_in_dim.44), channel_id=1, replica_groups=mesh['sp'=16,'dp'=8] {'sp'}, dimensions={0} | all-to-all | bytes 1048576 | tf_op jit(solution)/shard_map/all_to_all | solution.py:24
  42.9 18.8 %all_to_all.86 = bf16[16,256,128]{1,2,0:T(8,128)(2,1)} all-to-all(bf16[16,256,128]{1,2,0:T(8,128)(2,1)S(1)} %broadcast_in_dim.23), channel_id=1, replica_groups=mesh['sp'=16,'dp'=8] {'sp'}, dimensions={0} | all-to-all | bytes 2097152 | tf_op jit(solution)/shard_map/all_to_all | solution.py:24
  62.9 3.7 %all-to-all-start.7 = ((bf16[16,256,128]{1,2,0:T(8,128)(2,1)}), bf16[16,256,128]{1,2,0:T(8,128)(2,1)S(1)}, u32[]{:S(2)}, u32[]{:S(2)}) async-start(bf16[16,256,128]{1,2,0:T(8,128)(2,1)} %broadcast_in_dim.46), calls=%async_computation.7 | async-start | bytes 2097152 | tf_op jit(solution)/shard_map/all_to_all | solution.py:24
  67.0 3.5 %multiply_reduce_fusion.2 = (f32[256,8]{0,1:T(8,128)S(1)}, f32[256,8,128]{0,2,1:T(8,128)S(1)}) fusion(bf16[8,128,2048]{2,1,0:T(8,128)(2,1)} %bitcast.98, bf16[1,256,2048]{2,1,0:T(8,128)(2,1)S(1)} %copy-done), kind=kOutput, calls=%fused_computation.28 | convolution fusion | flops 1074264064 | bytes 6299648 | tf_op jit(solution)/shard_map/dot_general | solution.py:77
  72.0 1.6 gather_fusion
  73.7 7.9 %all-to-all-done.7 = bf16[16,256,128]{1,2,0:T(8,128)(2,1)S(1)} async-done(((bf16[16,256,128]{1,2,0:T(8,128)(2,1)}), bf16[16,256,128]{1,2,0:T(8,128)(2,1)S(1)}, u32[]{:S(2)}, u32[]{:S(2)}) %all-to-all-start.7) | async-done | bytes 1048608 | tf_op jit(solution)/shard_map/all_to_all | solution.py:24
  82.6 3.7 %all-to-all-start.3 = ((bf16[256,16,128]{2,0,1:T(8,128)(2,1)}), bf16[256,16,128]{2,0,1:T(8,128)(2,1)S(1)}, u32[]{:S(2)}, u32[]{:S(2)}) async-start(bf16[256,16,128]{2,0,1:T(8,128)(2,1)} %bitcast.17), calls=%async_computation.3 | async-start | bytes 2097152 | tf_op jit(solution)/shard_map/all_to_all | solution.py:109
  86.3 12.1 %all-gather.9.cloned.1.call-done = bf16[2048,1024]{0,1:T(8,128)(2,1)} async-done(((bf16[256,1024]{0,1:T(8,128)(2,1)}), bf16[2048,1024]{0,1:T(8,128)(2,1)}) %all-gather.9.cloned.1.call-update) | async-done | bytes 4194320 | tf_op jit(solution)/shard_map/all_gather | solution.py:79
  98.4 3.5 %fusion.11 = bf16[32,8,8,128]{3,2,1,0:T(8,128)(2,1)S(1)} fusion(bf16[2048,1024]{0,1:T(8,128)(2,1)} %all-gather.9.cloned.1.call-done, bf16[1,256,2048]{2,1,0:T(8,128)(2,1)S(1)} %copy-done), kind=kOutput, calls=%fused_computation.20 | convolution fusion | flops 1074003968 | bytes 5767168 | tf_op jit(solution)/shard_map/dot_general | solution.py:77
  101.9 1.7 gather_fusion.1
  103.6 50.8 %all-gather.5.cloned.1.call-done = bf16[2048,2048]{0,1:T(8,128)(2,1)} async-done(((bf16[256,2048]{0,1:T(8,128)(2,1)}), bf16[2048,2048]{0,1:T(8,128)(2,1)}) %all-gather.5.cloned.1.call-update) | async-done | bytes 8388624 | tf_op jit(solution)/shard_map/all_gather | solution.py:79
  154.4 7.2 %multiply_reduce_fusion.1 = (f32[256,16]{0,1:T(8,128)S(1)}, f32[256,16,128]{0,2,1:T(8,128)}) fusion(bf16[16,128,2048]{2,1,0:T(8,128)(2,1)} %bitcast.97, bf16[1,256,2048]{2,1,0:T(8,128)(2,1)S(1)} %copy-done), kind=kOutput, calls=%fused_computation.18 | convolution fusion | flops 2148528128 | bytes 11550720 | tf_op jit(solution)/shard_map/dot_general | solution.py:77
  161.6 7.1 %all-to-all-start.5 = ((bf16[256,16,128]{2,0,1:T(8,128)(2,1)}), bf16[256,16,128]{2,0,1:T(8,128)(2,1)}, u32[]{:S(2)}, u32[]{:S(2)}) async-start(bf16[256,16,128]{2,0,1:T(8,128)(2,1)} %bitcast.22), calls=%async_computation.5 | async-start | bytes 2097152 | tf_op jit(solution)/shard_map/all_to_all | solution.py:110
  168.7 3.3 %multiply_multiply_fusion = f32[256,16,128]{0,2,1:T(8,128)} fusion(f32[256,16,128]{0,2,1:T(8,128)} %get-tuple-element.56, f32[128]{0:T(128)S(1)} %get-tuple-element.52, f32[256,16]{0,1:T(8,128)S(1)} %add_rsqrt_fusion), kind=kLoop, calls=%fused_computation.17 | loop fusion | flops 1048576 | bytes 4211200 | tf_op jit(solution)/shard_map/mul | solution.py:44
  172.0 3.4 %reshape.170 = f32[256,16,64,2]{0,3,2,1:T(2,128)} reshape(f32[256,16,128]{0,2,1:T(8,128)} %multiply_multiply_fusion) | data formatting | bytes 4194304 | tf_op jit(solution)/shard_map/reshape | solution.py:46
  175.4 4.3 %subtract_convert_fusion = (bf16[256,16,64,1]{0,3,2,1:T(2,128)(2,1)S(1)}, bf16[256,16,64,1]{0,3,2,1:T(2,128)(2,1)S(1)}) fusion(f32[256,16,64,2]{0,3,2,1:T(2,128)} %reshape.170, f32[256,64]{0,1:T(8,128)S(1)} %get-tuple-element.50, f32[256,64]{0,1:T(8,128)S(1)} %get-tuple-element.49), kind=kLoop, calls=%fused_computation.30 | loop fusion | flops 2097152 | bytes 3276800 | tf_op jit(solution)/shard_map/convert.2
  179.7 2.4 pad_maximum_fusion
  183.9 2.7 all-to-all-done.5
  186.6 4.5 %all-to-all-start.1 = ((bf16[256,16,128]{2,0,1:T(8,128)(2,1)}), bf16[256,16,128]{2,0,1:T(8,128)(2,1)S(1)}, u32[]{:S(2)}, u32[]{:S(2)}) async-start(bf16[256,16,128]{2,0,1:T(8,128)(2,1)} %copy.20), calls=%async_computation.1 | async-start | bytes 2097152 | tf_op jit(solution)/shard_map/all_to_all | solution.py:102
  191.7 16.9 %all-to-all-done.1 = bf16[256,16,128]{2,0,1:T(8,128)(2,1)S(1)} async-done(((bf16[256,16,128]{2,0,1:T(8,128)(2,1)}), bf16[256,16,128]{2,0,1:T(8,128)(2,1)S(1)}, u32[]{:S(2)}, u32[]{:S(2)}) %all-to-all-start.1) | async-done | bytes 1048608 | tf_op jit(solution)/shard_map/all_to_all | solution.py:102
  208.6 47.3 %while.10 = (s32[]{:T(128)}, bf16[8,512,128]{2,1,0:T(8,128)(2,1)S(1)}, bf16[8,512,128]{2,1,0:T(8,128)(2,1)S(1)}, bf16[4096,128]{1,0:T(8,128)(2,1)S(1)}, bf16[4096,128]{1,0:T(8,128)(2,1)}, /*index=5*/s32[]{:T(128)}) while((s32[]{:T(128)}, bf16[8,512,128]{2,1,0:T(8,128)(2,1)S(1)}, bf16[8,512,128]{2,1,0:T(8,128)(2,1)S(1)}, ...), condition=%wide.region_5.6_spmd, body=%wide.region_2.5_spmd.sunk | while | flops 1092680704 | bytes 27535436 | solution.py:72
  208.6 1.3 multiply_reduce_fusion.4
  210.0 1.5 fusion.35
  211.5 3.1 %fusion.36 = bf16[8,512,128]{2,1,0:T(8,128)(2,1)S(1)} fusion(bf16[8,512,128]{2,1,0:T(8,128)(2,1)S(1)} %get-tuple-element.103, s32[]{:T(128)} %get-tuple-element.102, bf16[4096,128]{1,0:T(8,128)(2,1)} %get-tuple-element.112, f32[512,4096]{1,0:T(8,128)S(1)} %get-tuple-element.94, f32[512]{0:T(512)S(1)} %fusion.35, f32[512]{0:T(512)S(1)} %get-tuple-element.95), kind=kOutput, calls=%fused_computation.9.clone.1 | convolution fusion | flops 545325056 | bytes 9572356 | tf_op jit(solution)/shard_map/while/body/eval_jaxpr/dot_general | solution.py:68
  214.5 1.3 multiply_reduce_fusion.4
  215.9 1.5 fusion.35
  217.4 3.1 %fusion.36 = bf16[8,512,128]{2,1,0:T(8,128)(2,1)S(1)} fusion(bf16[8,512,128]{2,1,0:T(8,128)(2,1)S(1)} %get-tuple-element.103, s32[]{:T(128)} %get-tuple-element.102, bf16[4096,128]{1,0:T(8,128)(2,1)} %get-tuple-element.112, f32[512,4096]{1,0:T(8,128)S(1)} %get-tuple-element.94, f32[512]{0:T(512)S(1)} %fusion.35, f32[512]{0:T(512)S(1)} %get-tuple-element.95), kind=kOutput, calls=%fused_computation.9.clone.1 | convolution fusion | flops 545325056 | bytes 9572356 | tf_op jit(solution)/shard_map/while/body/eval_jaxpr/dot_general | solution.py:68
  220.5 1.3 multiply_reduce_fusion.4
  221.8 1.5 fusion.35
  223.3 3.1 %fusion.36 = bf16[8,512,128]{2,1,0:T(8,128)(2,1)S(1)} fusion(bf16[8,512,128]{2,1,0:T(8,128)(2,1)S(1)} %get-tuple-element.103, s32[]{:T(128)} %get-tuple-element.102, bf16[4096,128]{1,0:T(8,128)(2,1)} %get-tuple-element.112, f32[512,4096]{1,0:T(8,128)S(1)} %get-tuple-element.94, f32[512]{0:T(512)S(1)} %fusion.35, f32[512]{0:T(512)S(1)} %get-tuple-element.95), kind=kOutput, calls=%fused_computation.9.clone.1 | convolution fusion | flops 545325056 | bytes 9572356 | tf_op jit(solution)/shard_map/while/body/eval_jaxpr/dot_general | solution.py:68
  226.4 1.3 multiply_reduce_fusion.4
  227.7 1.5 fusion.35
  229.2 3.1 %fusion.36 = bf16[8,512,128]{2,1,0:T(8,128)(2,1)S(1)} fusion(bf16[8,512,128]{2,1,0:T(8,128)(2,1)S(1)} %get-tuple-element.103, s32[]{:T(128)} %get-tuple-element.102, bf16[4096,128]{1,0:T(8,128)(2,1)} %get-tuple-element.112, f32[512,4096]{1,0:T(8,128)S(1)} %get-tuple-element.94, f32[512]{0:T(512)S(1)} %fusion.35, f32[512]{0:T(512)S(1)} %get-tuple-element.95), kind=kOutput, calls=%fused_computation.9.clone.1 | convolution fusion | flops 545325056 | bytes 9572356 | tf_op jit(solution)/shard_map/while/body/eval_jaxpr/dot_general | solution.py:68
  232.3 1.3 multiply_reduce_fusion.4
  233.6 1.5 fusion.35
  235.1 3.1 %fusion.36 = bf16[8,512,128]{2,1,0:T(8,128)(2,1)S(1)} fusion(bf16[8,512,128]{2,1,0:T(8,128)(2,1)S(1)} %get-tuple-element.103, s32[]{:T(128)} %get-tuple-element.102, bf16[4096,128]{1,0:T(8,128)(2,1)} %get-tuple-element.112, f32[512,4096]{1,0:T(8,128)S(1)} %get-tuple-element.94, f32[512]{0:T(512)S(1)} %fusion.35, f32[512]{0:T(512)S(1)} %get-tuple-element.95), kind=kOutput, calls=%fused_computation.9.clone.1 | convolution fusion | flops 545325056 | bytes 9572356 | tf_op jit(solution)/shard_map/while/body/eval_jaxpr/dot_general | solution.py:68
  238.2 1.3 multiply_reduce_fusion.4
  239.6 1.5 fusion.35
  241.1 3.1 %fusion.36 = bf16[8,512,128]{2,1,0:T(8,128)(2,1)S(1)} fusion(bf16[8,512,128]{2,1,0:T(8,128)(2,1)S(1)} %get-tuple-element.103, s32[]{:T(128)} %get-tuple-element.102, bf16[4096,128]{1,0:T(8,128)(2,1)} %get-tuple-element.112, f32[512,4096]{1,0:T(8,128)S(1)} %get-tuple-element.94, f32[512]{0:T(512)S(1)} %fusion.35, f32[512]{0:T(512)S(1)} %get-tuple-element.95), kind=kOutput, calls=%fused_computation.9.clone.1 | convolution fusion | flops 545325056 | bytes 9572356 | tf_op jit(solution)/shard_map/while/body/eval_jaxpr/dot_general | solution.py:68
  244.2 1.3 multiply_reduce_fusion.4
  245.5 1.5 fusion.35
  247.0 3.1 %fusion.36 = bf16[8,512,128]{2,1,0:T(8,128)(2,1)S(1)} fusion(bf16[8,512,128]{2,1,0:T(8,128)(2,1)S(1)} %get-tuple-element.103, s32[]{:T(128)} %get-tuple-element.102, bf16[4096,128]{1,0:T(8,128)(2,1)} %get-tuple-element.112, f32[512,4096]{1,0:T(8,128)S(1)} %get-tuple-element.94, f32[512]{0:T(512)S(1)} %fusion.35, f32[512]{0:T(512)S(1)} %get-tuple-element.95), kind=kOutput, calls=%fused_computation.9.clone.1 | convolution fusion | flops 545325056 | bytes 9572356 | tf_op jit(solution)/shard_map/while/body/eval_jaxpr/dot_general | solution.py:68
  250.1 1.3 multiply_reduce_fusion.4
  251.4 1.5 fusion.35
  252.9 3.1 %fusion.36 = bf16[8,512,128]{2,1,0:T(8,128)(2,1)S(1)} fusion(bf16[8,512,128]{2,1,0:T(8,128)(2,1)S(1)} %get-tuple-element.103, s32[]{:T(128)} %get-tuple-element.102, bf16[4096,128]{1,0:T(8,128)(2,1)} %get-tuple-element.112, f32[512,4096]{1,0:T(8,128)S(1)} %get-tuple-element.94, f32[512]{0:T(512)S(1)} %fusion.35, f32[512]{0:T(512)S(1)} %get-tuple-element.95), kind=kOutput, calls=%fused_computation.9.clone.1 | convolution fusion | flops 545325056 | bytes 9572356 | tf_op jit(solution)/shard_map/while/body/eval_jaxpr/dot_general | solution.py:68
  256.0 19.4 %all_to_all.87 = bf16[16,256,128]{2,1,0:T(8,128)(2,1)S(1)} all-to-all(bf16[16,256,128]{2,1,0:T(8,128)(2,1)S(1)} %bitcast.95), channel_id=1, replica_groups=mesh['sp'=16,'dp'=8] {'sp'}, dimensions={0} | all-to-all | bytes 2097152 | tf_op jit(solution)/shard_map/all_to_all | solution.py:112
  276.0 6.7 %fusion.10 = bf16[1,256,2048]{2,1,0:T(8,128)(2,1)} fusion(bf16[256,2048]{0,1:T(8,128)(2,1)S(1)} %bitcast.96, bf16[2048,2048]{0,1:T(8,128)(2,1)} %all-gather.11.cloned.1.call-done), kind=kOutput, calls=%fused_computation.16 | convolution fusion | flops 2148007936 | bytes 10485760 | tf_op jit(solution)/shard_map/dot_general | solution.py:77
  (47 shorter events, 9.9 us)
Async XLA Ops:
  6.5 60.5 %copy-start = (bf16[1,256,2048]{2,1,0:T(8,128)(2,1)S(1)}, bf16[1,256,2048]{2,1,0:T(8,128)(2,1)}, u32[]{:S(2)}) copy-start(bf16[1,256,2048]{2,1,0:T(8,128)(2,1)} %param.11) | copy-start | bytes 3145732
  6.5 60.1 %copy-start.5 = (s32[16]{0:T(128)S(1)}, s32[16]{0:T(128)}, u32[]{:S(2)}) copy-start(s32[16]{0:T(128)} %constant.81) | copy-start | bytes 196
  6.5 55.2 %copy-start.3 = (bf16[256,128]{1,0:T(8,128)(2,1)S(1)}, bf16[256,128]{1,0:T(8,128)(2,1)}, u32[]{:S(2)}) copy-start(bf16[256,128]{1,0:T(8,128)(2,1)} %param.15) | copy-start | bytes 196612
  6.5 60.4 %copy-start.4 = (f32[2,128]{1,0:T(2,128)S(1)}, f32[2,128]{1,0:T(2,128)}, u32[]{:S(2)}) copy-start(f32[2,128]{1,0:T(2,128)} %param.16) | copy-start | bytes 3076
  6.5 60.5 %all-gather.7.cloned.1.call-start = ((), (), s32[]{:S(2)}) async-start(), calls=%async_computation.9 | async-start | bytes 4718592 | tf_op jit(solution)/shard_map/all_gather | solution.py:79
  27.1 71.3 %all-gather.9.cloned.1.call-start = ((), (), s32[]{:S(2)}) async-start(), calls=%async_computation.10 | async-start | bytes 4718592 | tf_op jit(solution)/shard_map/all_gather | solution.py:79
  41.8 112.6 %all-gather.5.cloned.1.call-start = ((), (), s32[]{:S(2)}) async-start(), calls=%async_computation.8 | async-start | bytes 9437184 | tf_op jit(solution)/shard_map/all_gather | solution.py:79
  62.9 18.6 %all-to-all-start.7 = ((bf16[16,256,128]{1,2,0:T(8,128)(2,1)}), bf16[16,256,128]{1,2,0:T(8,128)(2,1)S(1)}, u32[]{:S(2)}, u32[]{:S(2)}) async-start(bf16[16,256,128]{1,2,0:T(8,128)(2,1)} %broadcast_in_dim.46), calls=%async_computation.7 | async-start | bytes 2097152 | tf_op jit(solution)/shard_map/all_to_all | solution.py:24
  81.5 1.0 copy-start.2
  82.6 79.0 %all-to-all-start.3 = ((bf16[256,16,128]{2,0,1:T(8,128)(2,1)}), bf16[256,16,128]{2,0,1:T(8,128)(2,1)S(1)}, u32[]{:S(2)}, u32[]{:S(2)}) async-start(bf16[256,16,128]{2,0,1:T(8,128)(2,1)} %bitcast.17), calls=%async_computation.3 | async-start | bytes 2097152 | tf_op jit(solution)/shard_map/all_to_all | solution.py:109
  161.6 25.0 %all-to-all-start.5 = ((bf16[256,16,128]{2,0,1:T(8,128)(2,1)}), bf16[256,16,128]{2,0,1:T(8,128)(2,1)}, u32[]{:S(2)}, u32[]{:S(2)}) async-start(bf16[256,16,128]{2,0,1:T(8,128)(2,1)} %bitcast.22), calls=%async_computation.5 | async-start | bytes 2097152 | tf_op jit(solution)/shard_map/all_to_all | solution.py:110
  186.6 22.0 %all-to-all-start.1 = ((bf16[256,16,128]{2,0,1:T(8,128)(2,1)}), bf16[256,16,128]{2,0,1:T(8,128)(2,1)S(1)}, u32[]{:S(2)}, u32[]{:S(2)}) async-start(bf16[256,16,128]{2,0,1:T(8,128)(2,1)} %copy.20), calls=%async_computation.1 | async-start | bytes 2097152 | tf_op jit(solution)/shard_map/all_to_all | solution.py:102
  191.1 84.8 %all-gather.11.cloned.1.call-start = ((), (), s32[]{:S(2)}) async-start(), calls=%async_computation.11 | async-start | bytes 9437184 | tf_op jit(solution)/shard_map/all_gather | solution.py:79
  275.4 7.3 %copy-start.1 = (bf16[1,256,2048]{2,1,0:T(8,128)(2,1)S(1)}, bf16[1,256,2048]{2,1,0:T(8,128)(2,1)}, u32[]{:S(2)}) copy-start(bf16[1,256,2048]{2,1,0:T(8,128)(2,1)} %param.11) | copy-start | bytes 3145732
Sparse Core Ops, SparseCore 0:
  27.2 32.9 all-gather.6
  61.9 36.4 all-gather.8
  100.0 54.3 all-gather.4
  193.3 54.5 all-gather.10
where the time goes:
time: 290 us; the launch traced here: 289 us
  waiting for transfers between devices  91 us (31%)
  blocking collectives  71.7 us (25%)
  matrix products  56 us (19%)
  other arithmetic  22.9 us (8%)
  starting transfers between devices  19 us (7%)
  local copies, waits for them, and re-layouts  15.2 us (5%)
  between operations  13.4 us (5%)
    all_gather x4, waiting for transfers between devices, project(): lax.all_gather(col_full, 'dp', axis=0, tiled=True)  62.9 us
    all_to_all x3, blocking collectives, sent_to_all(): return lax.all_to_all(copies, axis, split_axis=0, concat_axis=0, tiled=True)  52.2 us
    dot_general x8, matrix products, one_block(): jnp.dot(probs_bf, value_rows, preferred_element_type=jnp.float32)  24.5 us
    dot_general x4, matrix products, project(): jnp.dot(own_rows, lax.all_gather(col_full, 'dp', axis=0, tiled=True), pre...  20.9 us
    all_to_all x1, blocking collectives, on_device(): lax.all_to_all(outputs, 'sp', split_axis=0, concat_axis=1, tiled=True)  19.4 us
    all_to_all x1, waiting for transfers between devices, on_device(): lax.all_to_all(prepare(raw_proj, qk_gain[0], cosine, sine_table).reshape(...  16.9 us
    reduce_sum x8, other arithmetic, one_block(): row_total = jnp.sum(weights, axis=1, keepdims=True)  12.1 us
    dot_general x8, matrix products, one_block(): jnp.dot(row_block, key_rows.T, preferred_element_type=jnp.float32)  10.7 us
  transfers between devices with their start and end apart: 8, of which 5 were waited for; matrix products, arithmetic and copies ran while one was open for 30% of the time, Pallas kernels for 0%

commit v1 on v0

--- a/solution.py
+++ b/solution.py
@@ -11,6 +11,22 @@
 GRID_W = 64
 ROPE_BASE = 10000.0
 EPS = 1e-06
+
+
+def ring_gather(x, axis, dim):
+    ways, here, lap = (lax.axis_size(axis), lax.axis_index(axis), x.shape[dim])
+    shape = [n * ways if d == dim else n for d, n in enumerate(x.shape)]
+    full = lax.dynamic_update_slice_in_dim(jnp.zeros(shape, x.dtype), x, here * lap, axis=dim)
+    going_up = going_down = x
+    for far in range(1, ways // 2 + 1):
+        going_up = lax.ppermute(going_up, axis, [(d, (d + 1) % ways) for d in range(ways)])
+        full = lax.dynamic_update_slice_in_dim(full, going_up, (here - far) % ways * lap, axis=dim)
+        if 2 * far < ways:
+            going_down = lax.ppermute(going_down, axis, [(d, (d - 1) % ways) for d in range(ways)])
+            full = lax.dynamic_update_slice_in_dim(
+                full, going_down, (here + far) % ways * lap, axis=dim
+            )
+    return full
 
 
 def in_order(blocks, dim):
@@ -74,11 +90,7 @@
 
 def project(own_rows, weight):
     col_full = collect(weight, "sp", 1)
-    return jnp.dot(
-        own_rows,
-        lax.all_gather(col_full, "dp", axis=0, tiled=True),
-        preferred_element_type=jnp.float32,
-    )
+    return jnp.dot(own_rows, ring_gather(col_full, "dp", 0), preferred_element_type=jnp.float32)
 
 
 def on_device(tokens, w_query, w_key, w_value, w_out, qk_gain):

time: 290 us -> 331 us (1.14)
  the two profiles are of different devices: /device:TPU:0 before, /device:TPU:7 now
where the time goes in v1:
time: 331 us; the launch traced here: 329 us
  local copies, waits for them, and re-layouts  96.2 us (29%)
  starting transfers between devices  69.4 us (21%)
  waiting for transfers between devices  56.7 us (17%)
  matrix products  53.8 us (16%)
  blocking collectives  31.3 us (9%)
  other arithmetic  21.3 us (6%)
    ppermute x16, starting transfers between devices, ring_gather(): lax.ppermute(going_up, axis, [(d, (d + 1) % ways) for d in range(ways)])  33.9 us
    all_to_all x2, blocking collectives, sent_to_all(): return lax.all_to_all(copies, axis, split_axis=0, concat_axis=0, tiled=True)  31.3 us
    dynamic_update_slice x15, local copies, waits for them, and re-layouts, ring_gather(): lax.dynamic_update_slice_in_dim(full, going_up, (here - far) % ways * lap...  28.5 us
    ppermute x16, waiting for transfers between devices, ring_gather(): lax.ppermute(going_up, axis, [(d, (d + 1) % ways) for d in range(ways)])  23.5 us
    dot_general x4, matrix products, project(): jnp.dot(own_rows, ring_gather(col_full, 'dp', 0), preferred_element_type=...  22.7 us
    dynamic_update_slice x12, local copies, waits for them, and re-layouts, ring_gather(): lax.dynamic_update_slice_in_dim(full, going_down, (here + far) % ways * l...  22.4 us
    dot_general x8, matrix products, one_block(): jnp.dot(probs_bf, value_rows, preferred_element_type=jnp.float32)  20.4 us
    all_to_all x2, waiting for transfers between devices, sent_to_all(): return lax.all_to_all(copies, axis, split_axis=0, concat_axis=0, tiled=True)  14.8 us
  transfers between devices with their start and end apart: 34, of which 8 were waited for; matrix products, arithmetic and copies ran while one was open for 48% of the time, Pallas kernels for 0%

profile of v1, /device:TPU:7, one launch (start us, length us, event | category | flops | bytes accessed | tf_op | source)
XLA Modules:
  0.0 329.4 jit_solution(11427762107101018924)
XLA Ops:
  0.9 18.1 %all_to_all.84 = bf16[16,256,64]{1,2,0:T(8,128)(2,1)} all-to-all(bf16[16,256,64]{1,2,0:T(8,128)(2,1)S(1)} %broadcast_in_dim.44), channel_id=1, replica_groups=mesh['sp'=16,'dp'=8] {'sp'}, dimensions={0} | all-to-all | bytes 1048576 | tf_op jit(solution)/shard_map/all_to_all | solution.py:40
  19.8 13.2 %all_to_all.85 = bf16[16,256,64]{1,2,0:T(8,128)(2,1)} all-to-all(bf16[16,256,64]{1,2,0:T(8,128)(2,1)S(1)} %broadcast_in_dim.42), channel_id=1, replica_groups=mesh['sp'=16,'dp'=8] {'sp'}, dimensions={0} | all-to-all | bytes 1048576 | tf_op jit(solution)/shard_map/all_to_all | solution.py:40
  35.1 3.7 %all-to-all-start = ((bf16[16,256,128]{2,1,0:T(8,128)(2,1)}), bf16[16,256,128]{2,1,0:T(8,128)(2,1)S(1)}, u32[]{:S(2)}, u32[]{:S(2)}) async-start(bf16[16,256,128]{2,1,0:T(8,128)(2,1)} %broadcast_in_dim.23), calls=%async_computation | async-start | bytes 2097152 | tf_op jit(solution)/shard_map/all_to_all | solution.py:40
  38.7 14.8 %all-to-all-done = bf16[16,256,128]{2,1,0:T(8,128)(2,1)S(1)} async-done(((bf16[16,256,128]{2,1,0:T(8,128)(2,1)}), bf16[16,256,128]{2,1,0:T(8,128)(2,1)S(1)}, u32[]{:S(2)}, u32[]{:S(2)}) %all-to-all-start) | async-done | bytes 1048608 | tf_op jit(solution)/shard_map/all_to_all | solution.py:40
  55.5 4.3 %all-to-all-start.7 = ((bf16[16,256,128]{2,1,0:T(8,128)(2,1)}), bf16[16,256,128]{2,1,0:T(8,128)(2,1)}, u32[]{:S(2)}, u32[]{:S(2)}) async-start(bf16[16,256,128]{2,1,0:T(8,128)(2,1)} %broadcast_in_dim.46), calls=%async_computation.7 | async-start | bytes 2097152 | tf_op jit(solution)/shard_map/all_to_all | solution.py:40
  59.9 3.8 %collective-permute-start.14 = (bf16[256,1024]{0,1:T(8,128)(2,1)}, bf16[256,1024]{0,1:T(8,128)(2,1)}, u32[]{:S(2)}, u32[]{:S(2)}) collective-permute-start(bf16[256,1024]{0,1:T(8,128)(2,1)} %bitcast.20), channel_id=1, source_target_pairs={{0,1},{1,2},{2,3},{3,4},{4,5},{5,6},{6,7},{7,0},{8,9},{9,10},{10,1... | collective-permute-start | bytes 1572872 | tf_op jit(solution)/shard_map/ppermute | solution.py:22
  63.8 3.0 collective-permute-start.7
  67.0 3.1 collective-permute-done.14
  70.1 3.7 %collective-permute-start.16 = (bf16[256,1024]{0,1:T(8,128)(2,1)}, bf16[256,1024]{0,1:T(8,128)(2,1)}, u32[]{:S(2)}, u32[]{:S(2)}) collective-permute-start(bf16[256,1024]{0,1:T(8,128)(2,1)} %collective-permute-done.14), channel_id=1, source_target_pairs={{0,1},{1,2},{2,3},{3,4},{4,5},{5,6},{6,7},{7,0},{8,9},{9,10},{10,1... | collective-permute-start | bytes 1572872 | tf_op jit(solution)/shard_map/ppermute | solution.py:22
  74.8 2.5 broadcast.157.clone
  79.8 2.5 broadcast.157.clone.1
  85.7 2.9 collective-permute-start.9
  88.6 4.3 %broadcast.154.clone = bf16[2048,2048]{0,1:T(8,128)(2,1)} broadcast(bf16[]{:T(256)} %constant.150.clone.1), dimensions={} | broadcast | bytes 8388610 | tf_op jit(solution)/shard_map/broadcast.8
  98.0 2.9 collective-permute-start.18
  106.7 2.9 collective-permute-start.11
  112.4 3.0 collective-permute-start.21
  116.3 3.0 collective-permute-start.2
  128.0 3.0 collective-permute-done.22
  131.0 13.0 %collective-permute-done.20 = bf16[256,1024]{0,1:T(8,128)(2,1)S(1)} collective-permute-done((bf16[256,1024]{0,1:T(8,128)(2,1)S(1)}, bf16[256,1024]{0,1:T(8,128)(2,1)S(1)}, u32[]{:S(2)}, u32[]{:S(2)}) %collective-permute-start.20) | collective-permute-done | bytes 524320 | tf_op jit(solution)/shard_map/ppermute | solution.py:22
  144.1 5.6 %collective-permute-done.13 = bf16[256,1024]{0,1:T(8,128)(2,1)S(1)} collective-permute-done((bf16[256,1024]{0,1:T(8,128)(2,1)S(1)}, bf16[256,1024]{0,1:T(8,128)(2,1)S(1)}, u32[]{:S(2)}, u32[]{:S(2)}) %collective-permute-start.13) | collective-permute-done | bytes 524320 | tf_op jit(solution)/shard_map/ppermute | solution.py:22
  150.8 3.7 %collective-permute-start.4 = (bf16[256,2048]{0,1:T(8,128)(2,1)}, bf16[256,2048]{0,1:T(8,128)(2,1)}, u32[]{:S(2)}, u32[]{:S(2)}) collective-permute-start(bf16[256,2048]{0,1:T(8,128)(2,1)} %collective-permute-done.2), channel_id=1, source_target_pairs={{0,1},{1,2},{2,3},{3,4},{4,5},{5,6},{6,7},{7,0},{8,9},{9,10},{10,1... | collective-permute-start | bytes 3145736 | tf_op jit(solution)/shard_map/ppermute | solution.py:22
  154.5 4.5 %bitcast_reduce_fusion.1 = (f32[256,8]{0,1:T(8,128)S(1)}, f32[256,1024]{0,1:T(8,128)}) fusion(bf16[2048,1024]{0,1:T(8,128)(2,1)} %get-tuple-element.62, bf16[1,256,2048]{2,1,0:T(8,128)(2,1)S(1)} %copy-done), kind=kOutput, calls=%fused_computation.23 | convolution fusion | flops 1074264064 | bytes 6299648 | tf_op jit(solution)/shard_map/dot_general | solution.py:93
  163.8 6.8 %all-to-all-start.3 = ((bf16[256,16,128]{2,0,1:T(8,128)(2,1)}), bf16[256,16,128]{2,0,1:T(8,128)(2,1)S(1)}, u32[]{:S(2)}, u32[]{:S(2)}) async-start(bf16[256,16,128]{2,0,1:T(8,128)(2,1)} %bitcast.88), calls=%async_computation.3 | async-start | bytes 2097152 | tf_op jit(solution)/shard_map/all_to_all | solution.py:121
  172.2 3.7 %collective-permute-start.6 = (bf16[256,2048]{0,1:T(8,128)(2,1)}, bf16[256,2048]{0,1:T(8,128)(2,1)}, u32[]{:S(2)}, u32[]{:S(2)}) collective-permute-start(bf16[256,2048]{0,1:T(8,128)(2,1)} %collective-permute-done.4), channel_id=1, source_target_pairs={{0,1},{1,2},{2,3},{3,4},{4,5},{5,6},{6,7},{7,0},{8,9},{9,10},{10,1... | collective-permute-start | bytes 3145736 | tf_op jit(solution)/shard_map/ppermute | solution.py:22
  175.9 4.3 %convolution_convert_fusion.1 = bf16[1024,256]{1,0:T(8,128)(2,1)} fusion(bf16[2048,1024]{0,1:T(8,128)(2,1)} %get-tuple-element.61, bf16[1,256,2048]{2,1,0:T(8,128)(2,1)S(1)} %copy-done), kind=kOutput, calls=%fused_computation.21 | convolution fusion | flops 1074003968 | bytes 5767168 | tf_op jit(solution)/shard_map/dot_general | solution.py:93
  180.2 2.7 gather_fusion.1
  194.7 7.2 %bitcast_reduce_fusion = (f32[256,16]{0,1:T(8,128)S(1)}, f32[256,2048]{0,1:T(8,128)}) fusion(bf16[2048,2048]{0,1:T(8,128)(2,1)} %constant_dynamic-update-slice_fusion.24, bf16[1,256,2048]{2,1,0:T(8,128)(2,1)S(1)} %copy-done), kind=kOutput, calls=%fused_computation.18 | convolution fusion | flops 2148528128 | bytes 11550720 | tf_op jit(solution)/shard_map/dot_general | solution.py:93
  201.8 3.4 %reshape.176 = f32[256,16,64,2]{0,3,2,1:T(2,128)} reshape(f32[256,2048]{0,1:T(8,128)} %get-tuple-element.56) | data formatting | bytes 4194304 | tf_op jit(solution)/shard_map/reshape | solution.py:113
  205.3 6.9 %all-to-all-start.5 = ((bf16[256,16,128]{0,2,1:T(8,128)(2,1)}), bf16[256,16,128]{0,2,1:T(8,128)(2,1)}, u32[]{:S(2)}, u32[]{:S(2)}) async-start(bf16[256,16,128]{0,2,1:T(8,128)(2,1)} %bitcast.87), calls=%async_computation.5 | async-start | bytes 2097152 | tf_op jit(solution)/shard_map/all_to_all | solution.py:122
  212.2 2.7 multiply_multiply_fusion
  214.9 2.9 subtract_convert_fusion
  217.8 2.4 pad_maximum_fusion
  223.7 4.7 %all-to-all-done.5 = bf16[256,16,128]{0,2,1:T(8,128)(2,1)} async-done(((bf16[256,16,128]{0,2,1:T(8,128)(2,1)}), bf16[256,16,128]{0,2,1:T(8,128)(2,1)}, u32[]{:S(2)}, u32[]{:S(2)}) %all-to-all-start.5) | async-done | bytes 1048608 | tf_op jit(solution)/shard_map/all_to_all | solution.py:122
  228.5 4.5 %all-to-all-start.1 = ((bf16[256,16,128]{2,0,1:T(8,128)(2,1)}), bf16[256,16,128]{2,0,1:T(8,128)(2,1)S(1)}, u32[]{:S(2)}, u32[]{:S(2)}) async-start(bf16[256,16,128]{2,0,1:T(8,128)(2,1)} %copy.28), calls=%async_computation.1 | async-start | bytes 2097152 | tf_op jit(solution)/shard_map/all_to_all | solution.py:114
  233.0 4.3 %broadcast.154.clone.1 = bf16[2048,2048]{0,1:T(8,128)(2,1)} broadcast(bf16[]{:T(256)} %constant.150.clone.1), dimensions={} | broadcast | bytes 8388610 | tf_op jit(solution)/shard_map/broadcast.8
  238.5 2.5 constant_dynamic-update-slice_fusion.6
  250.9 43.5 %while.10 = (s32[]{:T(128)}, bf16[8,512,128]{2,1,0:T(8,128)(2,1)S(1)}, bf16[8,512,128]{2,1,0:T(8,128)(2,1)S(1)}, bf16[4096,128]{1,0:T(8,128)(2,1)S(1)}, bf16[4096,128]{1,0:T(8,128)(2,1)}, /*index=5*/s32[]{:T(128)}) while((s32[]{:T(128)}, bf16[8,512,128]{2,1,0:T(8,128)(2,1)S(1)}, bf16[8,512,128]{2,1,0:T(8,128)(2,1)S(1)}, ...), condition=%wide.region_5.6_spmd, body=%wide.region_2.5_spmd.sunk | while | flops 1092680704 | bytes 31729776 | solution.py:88
  253.8 2.6 fusion.34
  259.2 2.6 fusion.34
  264.6 2.6 fusion.34
  270.1 2.6 fusion.34
  275.5 2.6 fusion.34
  281.0 2.6 fusion.34
  286.4 2.6 fusion.34
  291.8 2.6 fusion.34
  295.4 6.6 %all-to-all-start.6 = ((bf16[16,256,128]{2,1,0:T(8,128)(2,1)}), bf16[16,256,128]{2,1,0:T(8,128)(2,1)S(1)}, u32[]{:S(2)}, u32[]{:S(2)}) async-start(bf16[16,256,128]{2,1,0:T(8,128)(2,1)} %bitcast.93), calls=%async_computation.6 | async-start | bytes 2097152 | tf_op jit(solution)/shard_map/all_to_all | solution.py:124
  311.4 10.7 %all-to-all-done.6 = bf16[16,256,128]{2,1,0:T(8,128)(2,1)S(1)} async-done(((bf16[16,256,128]{2,1,0:T(8,128)(2,1)}), bf16[16,256,128]{2,1,0:T(8,128)(2,1)S(1)}, u32[]{:S(2)}, u32[]{:S(2)}) %all-to-all-start.6) | async-done | bytes 1048608 | tf_op jit(solution)/shard_map/all_to_all | solution.py:124
  322.6 6.7 %fusion.10 = bf16[1,256,2048]{2,1,0:T(8,128)(2,1)} fusion(bf16[256,2048]{0,1:T(8,128)(2,1)S(1)} %bitcast.95, bf16[2048,2048]{0,1:T(8,128)(2,1)} %constant_dynamic-update-slice_fusion), kind=kOutput, calls=%fused_computation.17 | convolution fusion | flops 2148007936 | bytes 10485760 | tf_op jit(solution)/shard_map/dot_general | solution.py:93
  (146 shorter events, 103.6 us)
Async XLA Ops:
  0.0 154.4 %copy-start = (bf16[1,256,2048]{2,1,0:T(8,128)(2,1)S(1)}, bf16[1,256,2048]{2,1,0:T(8,128)(2,1)}, u32[]{:S(2)}) copy-start(bf16[1,256,2048]{2,1,0:T(8,128)(2,1)} %param.11) | copy-start | bytes 3145732
  0.0 73.8 %copy-start.6 = (s32[16]{0:T(128)S(1)}, s32[16]{0:T(128)}, u32[]{:S(2)}) copy-start(s32[16]{0:T(128)} %constant.178) | copy-start | bytes 196
  0.0 66.7 %copy-start.5 = (f32[2,128]{1,0:T(2,128)S(1)}, f32[2,128]{1,0:T(2,128)}, u32[]{:S(2)}) copy-start(f32[2,128]{1,0:T(2,128)} %param.16) | copy-start | bytes 3076
  35.1 18.4 %all-to-all-start = ((bf16[16,256,128]{2,1,0:T(8,128)(2,1)}), bf16[16,256,128]{2,1,0:T(8,128)(2,1)S(1)}, u32[]{:S(2)}, u32[]{:S(2)}) async-start(bf16[16,256,128]{2,1,0:T(8,128)(2,1)} %broadcast_in_dim.23), calls=%async_computation | async-start | bytes 2097152 | tf_op jit(solution)/shard_map/all_to_all | solution.py:40
  55.5 28.7 %all-to-all-start.7 = ((bf16[16,256,128]{2,1,0:T(8,128)(2,1)}), bf16[16,256,128]{2,1,0:T(8,128)(2,1)}, u32[]{:S(2)}, u32[]{:S(2)}) async-start(bf16[16,256,128]{2,1,0:T(8,128)(2,1)} %broadcast_in_dim.46), calls=%async_computation.7 | async-start | bytes 2097152 | tf_op jit(solution)/shard_map/all_to_all | solution.py:40
  59.9 10.2 %collective-permute-start.14 = (bf16[256,1024]{0,1:T(8,128)(2,1)}, bf16[256,1024]{0,1:T(8,128)(2,1)}, u32[]{:S(2)}, u32[]{:S(2)}) collective-permute-start(bf16[256,1024]{0,1:T(8,128)(2,1)} %bitcast.20), channel_id=1, source_target_pairs={{0,1},{1,2},{2,3},{3,4},{4,5},{5,6},{6,7},{7,0},{8,9},{9,10},{10,1... | collective-permute-start | bytes 1572872 | tf_op jit(solution)/shard_map/ppermute | solution.py:22
  63.7 15.6 %collective-permute-start.15 = (bf16[256,1024]{0,1:T(8,128)(2,1)}, bf16[256,1024]{0,1:T(8,128)(2,1)}, u32[]{:S(2)}, u32[]{:S(2)}) collective-permute-start(bf16[256,1024]{0,1:T(8,128)(2,1)} %bitcast.20), channel_id=1, source_target_pairs={{0,7},{1,0},{2,1},{3,2},{4,3},{5,4},{6,5},{7,6},{8,15},{9,8},{10,9... | collective-permute-start | bytes 1572872 | tf_op jit(solution)/shard_map/ppermute | solution.py:25
  63.8 21.9 %collective-permute-start.7 = (bf16[256,1024]{0,1:T(8,128)(2,1)}, bf16[256,1024]{0,1:T(8,128)(2,1)}, u32[]{:S(2)}, u32[]{:S(2)}) collective-permute-start(bf16[256,1024]{0,1:T(8,128)(2,1)} %bitcast.11), channel_id=1, source_target_pairs={{0,1},{1,2},{2,3},{3,4},{4,5},{5,6},{6,7},{7,0},{8,9},{9,10},{10,1... | collective-permute-start | bytes 1572872 | tf_op jit(solution)/shard_map/ppermute | solution.py:22
  66.7 19.0 %collective-permute-start.8 = (bf16[256,1024]{0,1:T(8,128)(2,1)}, bf16[256,1024]{0,1:T(8,128)(2,1)}, u32[]{:S(2)}, u32[]{:S(2)}) collective-permute-start(bf16[256,1024]{0,1:T(8,128)(2,1)} %bitcast.11), channel_id=1, source_target_pairs={{0,7},{1,0},{2,1},{3,2},{4,3},{5,4},{6,5},{7,6},{8,15},{9,8},{10,9... | collective-permute-start | bytes 1572872 | tf_op jit(solution)/shard_map/ppermute | solution.py:25
  70.1 24.0 %collective-permute-start.16 = (bf16[256,1024]{0,1:T(8,128)(2,1)}, bf16[256,1024]{0,1:T(8,128)(2,1)}, u32[]{:S(2)}, u32[]{:S(2)}) collective-permute-start(bf16[256,1024]{0,1:T(8,128)(2,1)} %collective-permute-done.14), channel_id=1, source_target_pairs={{0,1},{1,2},{2,3},{3,4},{4,5},{5,6},{6,7},{7,0},{8,9},{9,10},{10,1... | collective-permute-start | bytes 1572872 | tf_op jit(solution)/shard_map/ppermute | solution.py:22
  74.8 34.9 %collective-permute-start = (bf16[256,2048]{0,1:T(8,128)(2,1)S(1)}, bf16[256,2048]{0,1:T(8,128)(2,1)}, u32[]{:S(2)}, u32[]{:S(2)}) collective-permute-start(bf16[256,2048]{0,1:T(8,128)(2,1)S(1)} %bitcast.84), channel_id=1, source_target_pairs={{0,1},{1,2},{2,3},{3,4},{4,5},{5,6},{6,7},{7,0},{8,9},{9,10},{10,1... | collective-permute-start | bytes 3145736 | tf_op jit(solution)/shard_map/ppermute | solution.py:22
  79.3 18.7 %collective-permute-start.17 = (bf16[256,1024]{0,1:T(8,128)(2,1)}, bf16[256,1024]{0,1:T(8,128)(2,1)}, u32[]{:S(2)}, u32[]{:S(2)}) collective-permute-start(bf16[256,1024]{0,1:T(8,128)(2,1)} %collective-permute-done.15), channel_id=1, source_target_pairs={{0,7},{1,0},{2,1},{3,2},{4,3},{5,4},{6,5},{7,6},{8,15},{9,8},{10,9... | collective-permute-start | bytes 1572872 | tf_op jit(solution)/shard_map/ppermute | solution.py:25
  85.7 26.7 %collective-permute-start.1 = (bf16[256,2048]{0,1:T(8,128)(2,1)S(1)}, bf16[256,2048]{0,1:T(8,128)(2,1)}, u32[]{:S(2)}, u32[]{:S(2)}) collective-permute-start(bf16[256,2048]{0,1:T(8,128)(2,1)S(1)} %bitcast.85), channel_id=1, source_target_pairs={{0,7},{1,0},{2,1},{3,2},{4,3},{5,4},{6,5},{7,6},{8,15},{9,8},{10,9... | collective-permute-start | bytes 3145736 | tf_op jit(solution)/shard_map/ppermute | solution.py:25
  85.7 17.1 %collective-permute-start.9 = (bf16[256,1024]{0,1:T(8,128)(2,1)}, bf16[256,1024]{0,1:T(8,128)(2,1)S(1)}, u32[]{:S(2)}, u32[]{:S(2)}) collective-permute-start(bf16[256,1024]{0,1:T(8,128)(2,1)} %collective-permute-done.7), channel_id=1, source_target_pairs={{0,1},{1,2},{2,3},{3,4},{4,5},{5,6},{6,7},{7,0},{8,9},{9,10},{10,1... | collective-permute-start | bytes 1572872 | tf_op jit(solution)/shard_map/ppermute | solution.py:22
  94.1 12.6 %collective-permute-start.10 = (bf16[256,1024]{0,1:T(8,128)(2,1)}, bf16[256,1024]{0,1:T(8,128)(2,1)S(1)}, u32[]{:S(2)}, u32[]{:S(2)}) collective-permute-start(bf16[256,1024]{0,1:T(8,128)(2,1)} %collective-permute-done.8), channel_id=1, source_target_pairs={{0,7},{1,0},{2,1},{3,2},{4,3},{5,4},{6,5},{7,6},{8,15},{9,8},{10,9... | collective-permute-start | bytes 1572872 | tf_op jit(solution)/shard_map/ppermute | solution.py:25
  98.0 17.4 %collective-permute-start.18 = (bf16[256,1024]{0,1:T(8,128)(2,1)}, bf16[256,1024]{0,1:T(8,128)(2,1)S(1)}, u32[]{:S(2)}, u32[]{:S(2)}) collective-permute-start(bf16[256,1024]{0,1:T(8,128)(2,1)} %collective-permute-done.16), channel_id=1, source_target_pairs={{0,1},{1,2},{2,3},{3,4},{4,5},{5,6},{6,7},{7,0},{8,9},{9,10},{10,1... | collective-permute-start | bytes 1572872 | tf_op jit(solution)/shard_map/ppermute | solution.py:22
  102.9 13.4 %collective-permute-start.19 = (bf16[256,1024]{0,1:T(8,128)(2,1)}, bf16[256,1024]{0,1:T(8,128)(2,1)S(1)}, u32[]{:S(2)}, u32[]{:S(2)}) collective-permute-start(bf16[256,1024]{0,1:T(8,128)(2,1)} %collective-permute-done.17), channel_id=1, source_target_pairs={{0,7},{1,0},{2,1},{3,2},{4,3},{5,4},{6,5},{7,6},{8,15},{9,8},{10,9... | collective-permute-start | bytes 1572872 | tf_op jit(solution)/shard_map/ppermute | solution.py:25
  106.7 14.9 %collective-permute-start.11 = (bf16[256,1024]{0,1:T(8,128)(2,1)S(1)}, bf16[256,1024]{0,1:T(8,128)(2,1)S(1)}, u32[]{:S(2)}, u32[]{:S(2)}) collective-permute-start(bf16[256,1024]{0,1:T(8,128)(2,1)S(1)} %collective-permute-done.9), channel_id=1, source_target_pairs={{0,1},{1,2},{2,3},{3,4},{4,5},{5,6},{6,7},{7,0},{8,9},{9,10},{10,1... | collective-permute-start | bytes 1572872 | tf_op jit(solution)/shard_map/ppermute | solution.py:22
  109.6 12.0 %collective-permute-start.12 = (bf16[256,1024]{0,1:T(8,128)(2,1)S(1)}, bf16[256,1024]{0,1:T(8,128)(2,1)S(1)}, u32[]{:S(2)}, u32[]{:S(2)}) collective-permute-start(bf16[256,1024]{0,1:T(8,128)(2,1)S(1)} %collective-permute-done.10), channel_id=1, source_target_pairs={{0,7},{1,0},{2,1},{3,2},{4,3},{5,4},{6,5},{7,6},{8,15},{9,8},{10,9... | collective-permute-start | bytes 1572872 | tf_op jit(solution)/shard_map/ppermute | solution.py:25
  112.4 15.1 %collective-permute-start.21 = (bf16[256,2048]{0,1:T(8,128)(2,1)S(1)}, bf16[256,2048]{0,1:T(8,128)(2,1)}, u32[]{:S(2)}, u32[]{:S(2)}) collective-permute-start(bf16[256,2048]{0,1:T(8,128)(2,1)S(1)} %bitcast.81), channel_id=1, source_target_pairs={{0,1},{1,2},{2,3},{3,4},{4,5},{5,6},{6,7},{7,0},{8,9},{9,10},{10,1... | collective-permute-start | bytes 3145736 | tf_op jit(solution)/shard_map/ppermute | solution.py:22
  115.5 15.5 %collective-permute-start.22 = (bf16[256,2048]{0,1:T(8,128)(2,1)S(1)}, bf16[256,2048]{0,1:T(8,128)(2,1)}, u32[]{:S(2)}, u32[]{:S(2)}) collective-permute-start(bf16[256,2048]{0,1:T(8,128)(2,1)S(1)} %bitcast.82), channel_id=1, source_target_pairs={{0,7},{1,0},{2,1},{3,2},{4,3},{5,4},{6,5},{7,6},{8,15},{9,8},{10,9... | collective-permute-start | bytes 3145736 | tf_op jit(solution)/shard_map/ppermute | solution.py:25
  116.3 34.4 %collective-permute-start.2 = (bf16[256,2048]{0,1:T(8,128)(2,1)}, bf16[256,2048]{0,1:T(8,128)(2,1)}, u32[]{:S(2)}, u32[]{:S(2)}) collective-permute-start(bf16[256,2048]{0,1:T(8,128)(2,1)} %collective-permute-done), channel_id=1, source_target_pairs={{0,1},{1,2},{2,3},{3,4},{4,5},{5,6},{6,7},{7,0},{8,9},{9,10},{10,1... | collective-permute-start | bytes 3145736 | tf_op jit(solution)/shard_map/ppermute | solution.py:22
  121.7 22.4 %collective-permute-start.20 = (bf16[256,1024]{0,1:T(8,128)(2,1)S(1)}, bf16[256,1024]{0,1:T(8,128)(2,1)S(1)}, u32[]{:S(2)}, u32[]{:S(2)}) collective-permute-start(bf16[256,1024]{0,1:T(8,128)(2,1)S(1)} %collective-permute-done.18), channel_id=1, source_target_pairs={{0,1},{1,2},{2,3},{3,4},{4,5},{5,6},{6,7},{7,0},{8,9},{9,10},{10,1... | collective-permute-start | bytes 1572872 | tf_op jit(solution)/shard_map/ppermute | solution.py:22
  121.7 28.0 %collective-permute-start.13 = (bf16[256,1024]{0,1:T(8,128)(2,1)S(1)}, bf16[256,1024]{0,1:T(8,128)(2,1)S(1)}, u32[]{:S(2)}, u32[]{:S(2)}) collective-permute-start(bf16[256,1024]{0,1:T(8,128)(2,1)S(1)} %collective-permute-done.11), channel_id=1, source_target_pairs={{0,1},{1,2},{2,3},{3,4},{4,5},{5,6},{6,7},{7,0},{8,9},{9,10},{10,1... | collective-permute-start | bytes 1572872 | tf_op jit(solution)/shard_map/ppermute | solution.py:22
  127.6 43.0 %collective-permute-start.3 = (bf16[256,2048]{0,1:T(8,128)(2,1)}, bf16[256,2048]{0,1:T(8,128)(2,1)}, u32[]{:S(2)}, u32[]{:S(2)}) collective-permute-start(bf16[256,2048]{0,1:T(8,128)(2,1)} %collective-permute-done.1), channel_id=1, source_target_pairs={{0,7},{1,0},{2,1},{3,2},{4,3},{5,4},{6,5},{7,6},{8,15},{9,8},{10,9... | collective-permute-start | bytes 3145736 | tf_op jit(solution)/shard_map/ppermute | solution.py:25
  131.0 51.9 %collective-permute-start.23 = (bf16[256,2048]{0,1:T(8,128)(2,1)}, bf16[256,2048]{0,1:T(8,128)(2,1)}, u32[]{:S(2)}, u32[]{:S(2)}) collective-permute-start(bf16[256,2048]{0,1:T(8,128)(2,1)} %collective-permute-done.21), channel_id=1, source_target_pairs={{0,1},{1,2},{2,3},{3,4},{4,5},{5,6},{6,7},{7,0},{8,9},{9,10},{10,1... | collective-permute-start | bytes 3145736 | tf_op jit(solution)/shard_map/ppermute | solution.py:22
  144.1 99.3 %collective-permute-start.24 = (bf16[256,2048]{0,1:T(8,128)(2,1)}, bf16[256,2048]{0,1:T(8,128)(2,1)}, u32[]{:S(2)}, u32[]{:S(2)}) collective-permute-start(bf16[256,2048]{0,1:T(8,128)(2,1)} %collective-permute-done.22), channel_id=1, source_target_pairs={{0,7},{1,0},{2,1},{3,2},{4,3},{5,4},{6,5},{7,6},{8,15},{9,8},{10,9... | collective-permute-start | bytes 3145736 | tf_op jit(solution)/shard_map/ppermute | solution.py:25
  150.8 21.5 %collective-permute-start.4 = (bf16[256,2048]{0,1:T(8,128)(2,1)}, bf16[256,2048]{0,1:T(8,128)(2,1)}, u32[]{:S(2)}, u32[]{:S(2)}) collective-permute-start(bf16[256,2048]{0,1:T(8,128)(2,1)} %collective-permute-done.2), channel_id=1, source_target_pairs={{0,1},{1,2},{2,3},{3,4},{4,5},{5,6},{6,7},{7,0},{8,9},{9,10},{10,1... | collective-permute-start | bytes 3145736 | tf_op jit(solution)/shard_map/ppermute | solution.py:22
  163.8 41.5 %all-to-all-start.3 = ((bf16[256,16,128]{2,0,1:T(8,128)(2,1)}), bf16[256,16,128]{2,0,1:T(8,128)(2,1)S(1)}, u32[]{:S(2)}, u32[]{:S(2)}) async-start(bf16[256,16,128]{2,0,1:T(8,128)(2,1)} %bitcast.88), calls=%async_computation.3 | async-start | bytes 2097152 | tf_op jit(solution)/shard_map/all_to_all | solution.py:121
  170.6 19.4 %collective-permute-start.5 = (bf16[256,2048]{0,1:T(8,128)(2,1)}, bf16[256,2048]{0,1:T(8,128)(2,1)}, u32[]{:S(2)}, u32[]{:S(2)}) collective-permute-start(bf16[256,2048]{0,1:T(8,128)(2,1)} %collective-permute-done.3), channel_id=1, source_target_pairs={{0,7},{1,0},{2,1},{3,2},{4,3},{5,4},{6,5},{7,6},{8,15},{9,8},{10,9... | collective-permute-start | bytes 3145736 | tf_op jit(solution)/shard_map/ppermute | solution.py:25
  172.2 20.1 %collective-permute-start.6 = (bf16[256,2048]{0,1:T(8,128)(2,1)}, bf16[256,2048]{0,1:T(8,128)(2,1)}, u32[]{:S(2)}, u32[]{:S(2)}) collective-permute-start(bf16[256,2048]{0,1:T(8,128)(2,1)} %collective-permute-done.4), channel_id=1, source_target_pairs={{0,1},{1,2},{2,3},{3,4},{4,5},{5,6},{6,7},{7,0},{8,9},{9,10},{10,1... | collective-permute-start | bytes 3145736 | tf_op jit(solution)/shard_map/ppermute | solution.py:22
  182.9 66.7 %collective-permute-start.25 = (bf16[256,2048]{0,1:T(8,128)(2,1)}, bf16[256,2048]{0,1:T(8,128)(2,1)}, u32[]{:S(2)}, u32[]{:S(2)}) collective-permute-start(bf16[256,2048]{0,1:T(8,128)(2,1)} %collective-permute-done.23), channel_id=1, source_target_pairs={{0,1},{1,2},{2,3},{3,4},{4,5},{5,6},{6,7},{7,0},{8,9},{9,10},{10,1... | collective-permute-start | bytes 3145736 | tf_op jit(solution)/shard_map/ppermute | solution.py:22
  205.3 23.2 %all-to-all-start.5 = ((bf16[256,16,128]{0,2,1:T(8,128)(2,1)}), bf16[256,16,128]{0,2,1:T(8,128)(2,1)}, u32[]{:S(2)}, u32[]{:S(2)}) async-start(bf16[256,16,128]{0,2,1:T(8,128)(2,1)} %bitcast.87), calls=%async_computation.5 | async-start | bytes 2097152 | tf_op jit(solution)/shard_map/all_to_all | solution.py:122
  228.5 22.5 %all-to-all-start.1 = ((bf16[256,16,128]{2,0,1:T(8,128)(2,1)}), bf16[256,16,128]{2,0,1:T(8,128)(2,1)S(1)}, u32[]{:S(2)}, u32[]{:S(2)}) async-start(bf16[256,16,128]{2,0,1:T(8,128)(2,1)} %copy.28), calls=%async_computation.1 | async-start | bytes 2097152 | tf_op jit(solution)/shard_map/all_to_all | solution.py:114
  238.5 12.4 %copy-start.2 = (bf16[8,512,128]{2,1,0:T(8,128)(2,1)S(1)}, bf16[8,512,128]{2,1,0:T(8,128)(2,1)}, u32[]{:S(2)}) copy-start(bf16[8,512,128]{2,1,0:T(8,128)(2,1)} %custom-call.4) | copy-start | bytes 3145732
  243.3 63.4 %collective-permute-start.26 = (bf16[256,2048]{0,1:T(8,128)(2,1)}, bf16[256,2048]{0,1:T(8,128)(2,1)}, u32[]{:S(2)}, u32[]{:S(2)}) collective-permute-start(bf16[256,2048]{0,1:T(8,128)(2,1)} %collective-permute-done.24), channel_id=1, source_target_pairs={{0,7},{1,0},{2,1},{3,2},{4,3},{5,4},{6,5},{7,6},{8,15},{9,8},{10,9... | collective-permute-start | bytes 3145736 | tf_op jit(solution)/shard_map/ppermute | solution.py:25
  249.6 59.5 %collective-permute-start.27 = (bf16[256,2048]{0,1:T(8,128)(2,1)}, bf16[256,2048]{0,1:T(8,128)(2,1)}, u32[]{:S(2)}, u32[]{:S(2)}) collective-permute-start(bf16[256,2048]{0,1:T(8,128)(2,1)} %collective-permute-done.25), channel_id=1, source_target_pairs={{0,1},{1,2},{2,3},{3,4},{4,5},{5,6},{6,7},{7,0},{8,9},{9,10},{10,1... | collective-permute-start | bytes 3145736 | tf_op jit(solution)/shard_map/ppermute | solution.py:22
  250.9 2.9 copy-start.4
  256.3 2.9 copy-start.4
  261.8 2.9 copy-start.4
  267.2 2.9 copy-start.4
  272.7 2.9 copy-start.4
  278.1 2.9 copy-start.4
  283.5 2.9 copy-start.4
  289.0 2.9 copy-start.4
  294.4 1.0 copy-start.3
  295.4 26.7 %all-to-all-start.6 = ((bf16[16,256,128]{2,1,0:T(8,128)(2,1)}), bf16[16,256,128]{2,1,0:T(8,128)(2,1)S(1)}, u32[]{:S(2)}, u32[]{:S(2)}) async-start(bf16[16,256,128]{2,1,0:T(8,128)(2,1)} %bitcast.93), calls=%async_computation.6 | async-start | bytes 2097152 | tf_op jit(solution)/shard_map/all_to_all | solution.py:124
  322.1 7.3 %copy-start.1 = (bf16[1,256,2048]{2,1,0:T(8,128)(2,1)S(1)}, bf16[1,256,2048]{2,1,0:T(8,128)(2,1)}, u32[]{:S(2)}) copy-start(bf16[1,256,2048]{2,1,0:T(8,128)(2,1)} %param.11) | copy-start | bytes 3145732
